TPU v7x, 512 devices: a whole 4x8x8 slice. The times are simulated.
512 devices in a mesh: rep: 2 (over z_hi), fs: 32 (over z_lo, y), tp: 8 (over x, core).
Axes of the slice: x: 4, y: 8, z: 8 (z_hi: 2, z_lo: 4; z = z_hi * 4 + z_lo), core: 2. Of those that a mesh axis runs over, the one named last changes fastest.
Arguments:
- x_later: bfloat16 [8192, 2048], P(('rep', 'fs')), may hold values from -6 to 6
- kept_input_rows: bfloat16 [8192, 2048], P(('rep', 'fs')), may hold values from -6 to 6
- cotangent: bfloat16 [8192, 2048], P(('rep', 'fs')), may hold values from -8 to 8
- norm_gain_vector: float32 [2048], replicated, may hold values from 0.1 to 1.9
- up_weight: bfloat16 [2048, 4096], P('fs', 'tp'), may hold values from -0.125 to 0.125
- down_weight: bfloat16 [4096, 2048], P('tp', 'fs'), may hold values from -0.09375 to 0.09375
- up_sum: float32 [2048, 4096], P('fs', 'tp'), may hold values from -6 to 6
- down_sum: float32 [4096, 2048], P('tp', 'fs'), may hold values from -6 to 6
Outputs:
- mixed: bfloat16 [8192, 2048], P(('rep', 'fs'))
- input_gradient_rows: bfloat16 [8192, 2048], P(('rep', 'fs'))
- up_total: float32 [2048, 4096], P('fs', 'tp')
- down_total: float32 [4096, 2048], P('tp', 'fs')
All inputs are finite; a program needn't handle non-finite values.
Results may differ from a plain program's by a relative error of at most 0.018.
Values may be sent and summed in bfloat16 or wider, within the bound.
No kernel may reach another device: no remote copies, remote signals or barrier semaphores. Data moves between devices by JAX's collectives and lax.ppermute only.
A program may use at most 64 MiB of HBM per device.

v0:
```python
import jax
import jax.numpy as jnp
from jax import lax
from jax.sharding import Mesh
from jax.sharding import PartitionSpec as P

FS = ("fs_0", "fs_1")
REP_FS = ("rep", "fs_0", "fs_1")
EPSILON = 1e-06
TRANSPOSED = (((1,), (1,)), ((), ()))
LEADING = (((0,), (0,)), ((), ()))


def sent_to_all(shard, axis):
    copies = jnp.broadcast_to(shard, (lax.axis_size(axis), *shard.shape))
    return lax.all_to_all(copies, axis, split_axis=0, concat_axis=0, tiled=True)


def in_order(tiles, dim):
    lengths = list(tiles.shape[1:])
    lengths[dim] *= tiles.shape[0]
    return jnp.moveaxis(tiles, 0, dim).reshape(lengths)


def gathered_copies(shard, axis, dim):
    tiles = sent_to_all(shard, axis)
    return in_order(tiles, dim)


def together(arrays, axis):
    ends = [0]
    for a in arrays:
        ends.append(ends[-1] + a.size)
    subtotal = lax.psum(jnp.concatenate([a.ravel() for a in arrays]), axis)
    return tuple((subtotal[b:e].reshape(a.shape) for a, b, e in zip(arrays, ends, ends[1:])))


def all_blocks(shard, axes, order):
    tiles = shard[None]
    for k in order:
        tiles = lax.all_gather(tiles, axes[k], axis=0, tiled=True)
    held = [lax.axis_size(axes[k]) for k in reversed(order)]
    tiles = tiles.reshape(*held, *shard.shape)
    turned = sorted(range(len(order)), key=lambda place: order[len(order) - 1 - place])
    return tiles.transpose(*turned, *range(len(order), tiles.ndim)).reshape(-1, *shard.shape)


def gathered_by_axis(shard, axes, order, dim):
    return in_order(all_blocks(shard, axes, order), dim)


def over_copies(shard, axis):
    return sent_to_all(shard, axis).astype(jnp.float32).sum(axis=0)


def norm_partial_terms(values, norm_gain_vector):
    floats = values.astype(jnp.float32)
    inverse = lax.rsqrt(jnp.mean(floats * floats, axis=-1, keepdims=True) + EPSILON)
    unit_rows = floats * inverse
    normed = (unit_rows * norm_gain_vector).astype(jnp.bfloat16)
    return (inverse, unit_rows, normed)


def squared_relu(pre_act):
    return jnp.square(jax.nn.relu(pre_act)).astype(jnp.bfloat16)


def body(
    x_later, kept_input_rows, cotangent, norm_gain_vector, up_weight, down_weight, up_sum, down_sum
):
    row_count = x_later.shape[0]
    grad_scale = float(row_count * lax.axis_size("rep") * lax.axis_size(FS)) ** (-0.5)
    inv_later, unit_later, normed_later = norm_partial_terms(x_later, norm_gain_vector)
    inverse_rms_kept, unit_kept_rows, normed_kept_rows = norm_partial_terms(
        kept_input_rows, norm_gain_vector
    )
    stacked = jnp.concatenate([normed_kept_rows, normed_later], axis=0)
    columns = stacked
    pre_act = jnp.dot(
        columns, gathered_copies(up_weight, FS, 0), preferred_element_type=jnp.float32
    )
    pre_saved = pre_act[:row_count]
    hidden_saved = squared_relu(pre_saved)
    hidden_later = squared_relu(pre_act[row_count:])
    shard_part = gathered_copies(down_weight, FS, 1)
    product = jnp.dot(hidden_later, shard_part, preferred_element_type=jnp.float32)
    columns = cotangent
    grad_acc = lax.dot_general(columns, shard_part, TRANSPOSED, preferred_element_type=jnp.float32)
    pre_grad = (grad_acc * 2.0 * jax.nn.relu(pre_saved)).astype(jnp.bfloat16)
    back_part = lax.dot_general(
        pre_grad, gathered_copies(up_weight, FS, 0), TRANSPOSED, preferred_element_type=jnp.float32
    )
    mixed_sum, back_sum = tuple(
        (
            part.astype(jnp.float32)
            for part in together(
                (product.astype(jnp.bfloat16), back_part.astype(jnp.bfloat16)), "tp"
            )
        )
    )
    mixed = mixed_sum.astype(jnp.bfloat16)
    scaled_rows = back_sum * norm_gain_vector
    input_gradient_rows = (
        inverse_rms_kept
        * (
            scaled_rows
            - unit_kept_rows * jnp.mean(scaled_rows * unit_kept_rows, axis=-1, keepdims=True)
        )
    ).astype(jnp.bfloat16)
    cot_columns, normed_columns = (
        lax.all_to_all(cotangent, FS, split_axis=1, concat_axis=0, tiled=True),
        lax.all_to_all(normed_kept_rows, FS, split_axis=1, concat_axis=0, tiled=True),
    )
    columns = normed_columns
    up_grad = grad_scale * lax.dot_general(
        columns,
        gathered_by_axis(pre_grad, FS, (0, 1), 0),
        LEADING,
        preferred_element_type=jnp.float32,
    )
    columns = cot_columns
    down_grad = lax.dot_general(
        gathered_by_axis(hidden_saved, FS, (0, 1), 0),
        columns,
        LEADING,
        preferred_element_type=jnp.float32,
    )
    up_added, down_added = (
        over_copies(up_grad.astype(jnp.bfloat16), "rep").astype(jnp.float32),
        over_copies((down_grad * grad_scale).astype(jnp.bfloat16), "rep").astype(jnp.float32),
    )
    return (mixed, input_gradient_rows, up_sum + up_added, down_sum + down_added)


def solution(mesh):
    finer = Mesh(
        mesh.devices.reshape(mesh.shape["rep"], 4, 8, mesh.shape["tp"]),
        ("rep", "fs_0", "fs_1", "tp"),
    )
    return jax.shard_map(
        body,
        mesh=finer,
        in_specs=(
            P(REP_FS, None),
            P(REP_FS, None),
            P(REP_FS, None),
            P(),
            P(FS, "tp"),
            P("tp", FS),
            P(FS, "tp"),
            P("tp", FS),
        ),
        out_specs=(P(REP_FS, None), P(REP_FS, None), P(FS, "tp"), P("tp", FS)),
        check_vma=False,
    )
```

profile of v0, /device:TPU:2, one launch (start us, length us, event | category | flops | bytes accessed | tf_op | source)
XLA Modules:
  0.0 325.3 jit_solution(14748956280166571231)
XLA Ops:
  8.0 1.1 broadcast_in_dim.12
  9.1 64.7 %all_to_all.59 = bf16[32,64,512]{2,1,0:T(8,128)(2,1)} all-to-all(bf16[32,64,512]{2,1,0:T(8,128)(2,1)S(1)} %broadcast_in_dim.12), channel_id=1, replica_groups=mesh['rep'=2,'fs_0'=4,'fs_1'=8,'tp'=8] {'fs_0','fs_1'}, dimensions={0} | all-to-all | bytes 4194304 | tf_op jit(solution)/shard_map/all_to_all | solution.py:16
  73.8 1.5 broadcast_in_dim.26
  75.3 4.5 %all-to-all-start.1 = ((bf16[32,512,64]{1,2,0:T(8,128)(2,1)}), bf16[32,512,64]{1,2,0:T(8,128)(2,1)S(1)}, u32[]{:S(2)}, u32[]{:S(2)}) async-start(bf16[32,512,64]{1,2,0:T(8,128)(2,1)} %broadcast_in_dim.26), calls=%async_computation.1 | async-start | bytes 4194304 | tf_op jit(solution)/shard_map/all_to_all | solution.py:16
  79.8 0.0 all-reduce.2.cloned.1.call-start
  79.9 0.2 fusion.14
  80.1 0.2 fusion.15
  80.3 0.3 fusion.9
  80.6 0.8 copy-done.8
  81.4 0.1 copy-done.1
  81.5 1.5 fusion.18
  83.0 51.5 %all-to-all-done.1 = bf16[32,512,64]{1,2,0:T(8,128)(2,1)S(1)} async-done(((bf16[32,512,64]{1,2,0:T(8,128)(2,1)}), bf16[32,512,64]{1,2,0:T(8,128)(2,1)S(1)}, u32[]{:S(2)}, u32[]{:S(2)}) %all-to-all-start.1) | async-done | bytes 2097184 | tf_op jit(solution)/shard_map/all_to_all | solution.py:16
  134.5 1.8 fusion.3
  136.4 0.5 fusion.6
  136.8 1.1 copy-done.2
  137.9 0.8 fusion.4
  138.8 0.1 copy.43
  138.9 0.1 copy.42
  139.0 1.1 pad_maximum_fusion
  140.1 0.0 all-gather.5.cloned.1.call-start
  140.2 15.7 %all-gather = bf16[512,512]{1,0:T(8,128)(2,1)} all-gather(bf16[128,512]{1,0:T(8,128)(2,1)S(1)} %fusion.6), channel_id=2, replica_groups=mesh['rep'=2,'fs_0'=4,'fs_1'=8,'tp'=8] {'fs_0'}, dimensions={0}, use_global_device_ids=true | all-gather | bytes 655360 | tf_op jit(solution)/shard_map/all_gather | solution.py:41
  155.9 0.0 all-gather.5.cloned.1.call-update
  155.9 1.0 copy.34
  156.9 5.6 %all-to-all-start.2 = ((bf16[128,32,64]{0,2,1:T(8,128)(2,1)}), bf16[128,32,64]{0,2,1:T(8,128)(2,1)S(1)}, u32[]{:S(2)}, u32[]{:S(2)}) async-start(bf16[128,32,64]{0,2,1:T(8,128)(2,1)} %bitcast.4), calls=%async_computation.2 | async-start | bytes 1048576 | tf_op jit(solution)/shard_map/all_to_all | solution.py:112
  162.5 0.0 all-gather.7.cloned.1.call-start
  162.5 1.0 copy.38
  163.6 21.1 %all-gather.1 = bf16[512,512]{1,0:T(8,128)(2,1)} all-gather(bf16[128,512]{1,0:T(8,128)(2,1)S(1)} %multiply_convert_fusion), channel_id=3, replica_groups=mesh['rep'=2,'fs_0'=4,'fs_1'=8,'tp'=8] {'fs_0'}, dimensions={0}, use_global_device_ids=true | all-gather | bytes 655360 | tf_op jit(solution)/shard_map/all_gather | solution.py:41
  184.8 8.8 %all-to-all-start.4 = ((bf16[128,32,64]{0,2,1:T(8,128)(2,1)}), bf16[128,32,64]{0,2,1:T(8,128)(2,1)}, u32[]{:S(2)}, u32[]{:S(2)}) async-start(bf16[128,32,64]{0,2,1:T(8,128)(2,1)} %bitcast.14), calls=%async_computation.4 | async-start | bytes 1048576 | tf_op jit(solution)/shard_map/all_to_all | solution.py:111
  193.5 16.0 %all-reduce.2.cloned.1.call-done = bf16[524288]{0:T(1024)(128)(2,1)} async-done(((bf16[524288]{0:T(1024)(128)(2,1)}), bf16[524288]{0:T(1024)(128)(2,1)}) %all-reduce.2.cloned.1.call-update) | async-done | bytes 1048592 | tf_op jit(solution)/shard_map/psum | solution.py:34
  209.6 2.1 slice_convert_fusion
  211.7 0.2 reshape.80
  211.8 0.3 fusion.10
  212.1 12.9 %all-gather.5.cloned.1.call-done = bf16[32,128,512]{2,1,0:T(8,128)(2,1)} async-done(((bf16[4,128,512]{2,1,0:T(8,128)(2,1)}), bf16[32,128,512]{2,1,0:T(8,128)(2,1)}) %all-gather.5.cloned.1.call-update) | async-done | bytes 4194320 | tf_op jit(solution)/shard_map/all_gather | solution.py:41
  225.0 4.6 %copy.36 = bf16[4,8,128,512]{3,2,1,0:T(8,128)(2,1)} copy(bf16[4,8,128,512]{3,2,0,1:T(8,128)(2,1)} %bitcast.52) | data formatting | bytes 8388608 | tf_op jit(solution)/shard_map/transpose | solution.py:45
  229.6 53.1 %all-gather.7.cloned.1.call-done = bf16[32,128,512]{2,1,0:T(8,128)(2,1)} async-done(((bf16[4,128,512]{2,1,0:T(8,128)(2,1)}), bf16[32,128,512]{2,1,0:T(8,128)(2,1)}) %all-gather.7.cloned.1.call-update) | async-done | bytes 4194320 | tf_op jit(solution)/shard_map/all_gather | solution.py:41
  282.8 4.7 %copy.37 = bf16[4,8,128,512]{3,2,1,0:T(8,128)(2,1)} copy(bf16[4,8,128,512]{3,2,0,1:T(8,128)(2,1)} %bitcast.53) | data formatting | bytes 8388608 | tf_op jit(solution)/shard_map/transpose | solution.py:45
  287.5 0.8 fusion.7
  288.3 0.7 broadcast_in_dim.28
  289.0 7.4 %all-to-all-start.3 = ((bf16[2,64,512]{2,1,0:T(8,128)(2,1)}), bf16[2,64,512]{2,1,0:T(8,128)(2,1)S(1)}, u32[]{:S(2)}, u32[]{:S(2)}) async-start(bf16[2,64,512]{2,1,0:T(8,128)(2,1)} %broadcast_in_dim.28), calls=%async_computation.3 | async-start | bytes 262144 | tf_op jit(solution)/shard_map/all_to_all | solution.py:16
  296.4 3.2 fusion.8
  299.6 5.2 %all-to-all-done.3 = bf16[2,64,512]{2,1,0:T(8,128)(2,1)S(1)} async-done(((bf16[2,64,512]{2,1,0:T(8,128)(2,1)}), bf16[2,64,512]{2,1,0:T(8,128)(2,1)S(1)}, u32[]{:S(2)}, u32[]{:S(2)}) %all-to-all-start.3) | async-done | bytes 131104 | tf_op jit(solution)/shard_map/all_to_all | solution.py:16
  304.8 0.7 broadcast_in_dim.30
  305.4 3.4 %all-to-all-start.5 = ((bf16[2,512,64]{1,2,0:T(8,128)(2,1)}), bf16[2,512,64]{1,2,0:T(8,128)(2,1)S(1)}, u32[]{:S(2)}, u32[]{:S(2)}) async-start(bf16[2,512,64]{1,2,0:T(8,128)(2,1)} %broadcast_in_dim.30), calls=%async_computation.5 | async-start | bytes 262144 | tf_op jit(solution)/shard_map/all_to_all | solution.py:16
  308.8 1.1 fusion.13
  310.0 1.0 slice.33
  311.0 0.7 add.26
  311.7 5.5 %all-to-all-done.5 = bf16[2,512,64]{1,2,0:T(8,128)(2,1)S(1)} async-done(((bf16[2,512,64]{1,2,0:T(8,128)(2,1)}), bf16[2,512,64]{1,2,0:T(8,128)(2,1)S(1)}, u32[]{:S(2)}, u32[]{:S(2)}) %all-to-all-start.5) | async-done | bytes 131104 | tf_op jit(solution)/shard_map/all_to_all | solution.py:16
  317.2 0.7 add.27
  (38 shorter events, 0.2 us)
Async XLA Ops:
  9.1 64.7 %copy-start.15 = (bf16[512,64]{0,1:T(8,128)(2,1)S(1)}, bf16[512,64]{0,1:T(8,128)(2,1)}, u32[]{:S(2)}) copy-start(bf16[512,64]{0,1:T(8,128)(2,1)} %param.13) | copy-start | bytes 196612
  75.3 4.6 %copy-start.3 = (bf16[128,2048]{1,0:T(8,128)(2,1)S(1)}, bf16[128,2048]{1,0:T(8,128)(2,1)}, u32[]{:S(2)}) copy-start(bf16[128,2048]{1,0:T(8,128)(2,1)} %param.9) | copy-start | bytes 1572868
  75.3 4.8 %copy-start.5 = (bf16[128,2048]{1,0:T(8,128)(2,1)S(1)}, bf16[128,2048]{1,0:T(8,128)(2,1)}, u32[]{:S(2)}) copy-start(bf16[128,2048]{1,0:T(8,128)(2,1)} %param.8) | copy-start | bytes 1572868
  75.3 5.0 %copy-start.14 = (f32[2048]{0:T(1024)S(1)}, f32[2048]{0:T(1024)}, u32[]{:S(2)}) copy-start(f32[2048]{0:T(1024)} %param.11) | copy-start | bytes 24580
  75.3 59.2 %all-to-all-start.1 = ((bf16[32,512,64]{1,2,0:T(8,128)(2,1)}), bf16[32,512,64]{1,2,0:T(8,128)(2,1)S(1)}, u32[]{:S(2)}, u32[]{:S(2)}) async-start(bf16[32,512,64]{1,2,0:T(8,128)(2,1)} %broadcast_in_dim.26), calls=%async_computation.1 | async-start | bytes 4194304 | tf_op jit(solution)/shard_map/all_to_all | solution.py:16
  79.8 129.7 %all-reduce.2.cloned.1.call-start = ((), (), s32[]{:S(2)}) async-start(), calls=%async_computation.6 | async-start | bytes 2097152 | tf_op jit(solution)/shard_map/psum | solution.py:34
  79.9 1.6 copy-start.1
  80.6 0.8 copy-start.8
  83.0 53.4 %copy-start.6 = (bf16[128,2048]{1,0:T(8,128)(2,1)S(1)}, bf16[128,2048]{1,0:T(8,128)(2,1)}, u32[]{:S(2)}) copy-start(bf16[128,2048]{1,0:T(8,128)(2,1)} %param.10) | copy-start | bytes 1572868
  134.5 1.9 copy-start.10
  136.3 1.6 copy-start.2
  139.0 16.9 %copy-start.9 = (bf16[128,2048]{1,0:T(8,128)(2,1)S(1)}, bf16[128,2048]{1,0:T(8,128)(2,1)}, u32[]{:S(2)}) copy-start(bf16[128,2048]{1,0:T(8,128)(2,1)} %copy-done.8) | copy-start | bytes 1572868
  140.1 22.5 %copy-start.7 = (bf16[128,2048]{1,0:T(8,128)(2,1)S(1)}, bf16[128,2048]{1,0:T(8,128)(2,1)}, u32[]{:S(2)}) copy-start(bf16[128,2048]{1,0:T(8,128)(2,1)} %param.10) | copy-start | bytes 1572868
  140.1 23.5 %copy-start.11 = (f32[256,512]{1,0:T(8,128)S(1)}, f32[256,512]{1,0:T(8,128)}, u32[]{:S(2)}) copy-start(f32[256,512]{1,0:T(8,128)} %fusion.18) | copy-start | bytes 1572868
  140.1 84.9 %all-gather.5.cloned.1.call-start = ((), (), s32[]{:S(2)}) async-start(), calls=%async_computation.7 | async-start | bytes 4718592 | tf_op jit(solution)/shard_map/all_gather | solution.py:41
  156.9 27.9 %all-to-all-start.2 = ((bf16[128,32,64]{0,2,1:T(8,128)(2,1)}), bf16[128,32,64]{0,2,1:T(8,128)(2,1)S(1)}, u32[]{:S(2)}, u32[]{:S(2)}) async-start(bf16[128,32,64]{0,2,1:T(8,128)(2,1)} %bitcast.4), calls=%async_computation.2 | async-start | bytes 1048576 | tf_op jit(solution)/shard_map/all_to_all | solution.py:112
  162.5 120.3 %all-gather.7.cloned.1.call-start = ((), (), s32[]{:S(2)}) async-start(), calls=%async_computation.8 | async-start | bytes 4718592 | tf_op jit(solution)/shard_map/all_gather | solution.py:41
  184.8 103.6 %all-to-all-start.4 = ((bf16[128,32,64]{0,2,1:T(8,128)(2,1)}), bf16[128,32,64]{0,2,1:T(8,128)(2,1)}, u32[]{:S(2)}, u32[]{:S(2)}) async-start(bf16[128,32,64]{0,2,1:T(8,128)(2,1)} %bitcast.14), calls=%async_computation.4 | async-start | bytes 1048576 | tf_op jit(solution)/shard_map/all_to_all | solution.py:111
  282.8 4.7 %copy-start = (bf16[4,8,128,512]{3,2,1,0:T(8,128)(2,1)S(1)}, bf16[4,8,128,512]{3,2,1,0:T(8,128)(2,1)}, u32[]{:S(2)}) copy-start(bf16[4,8,128,512]{3,2,1,0:T(8,128)(2,1)} %copy.36) | copy-start | bytes 12582916
  289.0 15.7 %all-to-all-start.3 = ((bf16[2,64,512]{2,1,0:T(8,128)(2,1)}), bf16[2,64,512]{2,1,0:T(8,128)(2,1)S(1)}, u32[]{:S(2)}, u32[]{:S(2)}) async-start(bf16[2,64,512]{2,1,0:T(8,128)(2,1)} %broadcast_in_dim.28), calls=%async_computation.3 | async-start | bytes 262144 | tf_op jit(solution)/shard_map/all_to_all | solution.py:16
  299.6 10.4 %copy-start.4 = (bf16[262144]{0:T(1024)(128)(2,1)S(1)}, bf16[262144]{0:T(1024)(128)(2,1)}, u32[]{:S(2)}) copy-start(bf16[262144]{0:T(1024)(128)(2,1)} %get-tuple-element.9) | copy-start | bytes 1572868
  299.6 11.4 %copy-start.12 = (f32[64,512]{1,0:T(8,128)S(1)}, f32[64,512]{1,0:T(8,128)}, u32[]{:S(2)}) copy-start(f32[64,512]{1,0:T(8,128)} %param.14) | copy-start | bytes 393220
  305.4 11.8 %all-to-all-start.5 = ((bf16[2,512,64]{1,2,0:T(8,128)(2,1)}), bf16[2,512,64]{1,2,0:T(8,128)(2,1)S(1)}, u32[]{:S(2)}, u32[]{:S(2)}) async-start(bf16[2,512,64]{1,2,0:T(8,128)(2,1)} %broadcast_in_dim.30), calls=%async_computation.5 | async-start | bytes 262144 | tf_op jit(solution)/shard_map/all_to_all | solution.py:16
  308.8 8.4 %copy-start.13 = (f32[512,64]{0,1:T(8,128)S(1)}, f32[512,64]{0,1:T(8,128)}, u32[]{:S(2)}) copy-start(f32[512,64]{0,1:T(8,128)} %param.15) | copy-start | bytes 393220
Sparse Core Ops, SparseCore 0:
  140.2 69.2 all-reduce.1
Sparse Core Ops, SparseCore 1:
  156.0 69.0 all-gather.4
  227.0 55.7 all-gather.6
where the time goes:
time: 326 us; the launch traced here: 325 us
  waiting for transfers between devices  144 us (44%)
  blocking collectives  101 us (31%)
  starting transfers between devices  29.7 us (9%)
  local copies, waits for them, and re-layouts  18.8 us (6%)
  between operations  15.8 us (5%)
  matrix products  8.61 us (3%)
  other arithmetic  6.7 us (2%)
    all_gather x2, waiting for transfers between devices, all_blocks(): tiles = lax.all_gather(tiles, axes[k], axis=0, tiled=True)  66 us
    all_to_all x1, blocking collectives, sent_to_all(): return lax.all_to_all(copies, axis, split_axis=0, concat_axis=0, tiled=True)  64.7 us
    all_to_all x3, waiting for transfers between devices, sent_to_all(): return lax.all_to_all(copies, axis, split_axis=0, concat_axis=0, tiled=True)  62.2 us
    all_gather x2, blocking collectives, all_blocks(): tiles = lax.all_gather(tiles, axes[k], axis=0, tiled=True)  36.8 us
    psum x1, waiting for transfers between devices, together(): subtotal = lax.psum(jnp.concatenate([a.ravel() for a in arrays]), axis)  16 us
    all_to_all x3, starting transfers between devices, sent_to_all(): return lax.all_to_all(copies, axis, split_axis=0, concat_axis=0, tiled=True)  15.2 us
    transpose x2, local copies, waits for them, and re-layouts, all_blocks(): tiles.transpose(*turned, *range(len(order), tiles.ndim))  9.32 us
    all_to_all x1, starting transfers between devices, body(): lax.all_to_all(cotangent, FS, split_axis=1, concat_axis=0, tiled=True)  8.76 us
  transfers between devices with their start and end apart: 8, of which 6 were waited for; matrix products, arithmetic and copies ran while one was open for 7% of the time, Pallas kernels for 0%

commit v1 on v0

--- a/solution.py
+++ b/solution.py
@@ -38,7 +38,9 @@
 def all_blocks(shard, axes, order):
     tiles = shard[None]
     for k in order:
-        tiles = lax.all_gather(tiles, axes[k], axis=0, tiled=True)
+        tiles = jnp.concatenate(
+            lax.all_to_all(jnp.stack([tiles] * lax.axis_size(axes[k])), axes[k], 0, 0), axis=0
+        )
     held = [lax.axis_size(axes[k]) for k in reversed(order)]
     tiles = tiles.reshape(*held, *shard.shape)
     turned = sorted(range(len(order)), key=lambda place: order[len(order) - 1 - place])

time: 326 us -> 458 us (1.40)
  the two profiles are of different devices: /device:TPU:2 before, /device:TPU:14 now
where the time goes in v1:
time: 458 us; the launch traced here: 456 us
  waiting for transfers between devices  272 us (59%)
  blocking collectives  79.9 us (17%)
  starting transfers between devices  46 us (10%)
  local copies, waits for them, and re-layouts  25.3 us (6%)
  between operations  14.3 us (3%)
  matrix products  10.4 us (2%)
  other arithmetic  8.58 us (2%)
    all_to_all x3, waiting for transfers between devices, all_blocks(): lax.all_to_all(jnp.stack([tiles] * lax.axis_size(axes[k])), axes[k], 0, 0)  194 us
    all_to_all x1, blocking collectives, sent_to_all(): return lax.all_to_all(copies, axis, split_axis=0, concat_axis=0, tiled=True)  64.2 us
    all_to_all x3, waiting for transfers between devices, sent_to_all(): return lax.all_to_all(copies, axis, split_axis=0, concat_axis=0, tiled=True)  58.6 us
    all_to_all x3, starting transfers between devices, all_blocks(): lax.all_to_all(jnp.stack([tiles] * lax.axis_size(axes[k])), axes[k], 0, 0)  16.7 us
    all_to_all x3, starting transfers between devices, sent_to_all(): return lax.all_to_all(copies, axis, split_axis=0, concat_axis=0, tiled=True)  16.1 us
    all_to_all x1, blocking collectives, all_blocks(): lax.all_to_all(jnp.stack([tiles] * lax.axis_size(axes[k])), axes[k], 0, 0)  15.6 us
    all_to_all x1, waiting for transfers between devices, body(): lax.all_to_all(normed_kept_rows, FS, split_axis=1, concat_axis=0, tiled=T...  13.3 us
  transfers between devices with their start and end apart: 9, of which 8 were waited for; matrix products, arithmetic and copies ran while one was open for 7% of the time, Pallas kernels for 0%

profile of v1, /device:TPU:14, one launch (start us, length us, event | category | flops | bytes accessed | tf_op | source)
XLA Modules:
  0.0 456.5 jit_solution(7557668740248413795)
XLA Ops:
  7.2 1.1 broadcast_in_dim.8
  8.3 64.2 %all_to_all.79 = bf16[32,64,512]{2,1,0:T(8,128)(2,1)} all-to-all(bf16[32,64,512]{2,1,0:T(8,128)(2,1)S(1)} %broadcast_in_dim.8), channel_id=1, replica_groups=mesh['rep'=2,'fs_0'=4,'fs_1'=8,'tp'=8] {'fs_0','fs_1'}, dimensions={0} | all-to-all | bytes 4194304 | tf_op jit(solution)/shard_map/all_to_all | solution.py:16
  72.5 1.6 broadcast_in_dim.9
  74.1 5.1 %all-to-all-start.1 = ((bf16[32,512,64]{1,2,0:T(8,128)(2,1)}), bf16[32,512,64]{1,2,0:T(8,128)(2,1)S(1)}, u32[]{:S(2)}, u32[]{:S(2)}) async-start(bf16[32,512,64]{1,2,0:T(8,128)(2,1)} %broadcast_in_dim.9), calls=%async_computation.1 | async-start | bytes 4194304 | tf_op jit(solution)/shard_map/all_to_all | solution.py:16
  79.2 0.2 fusion.14
  79.4 0.2 fusion.15
  79.6 1.3 fusion.9
  80.9 2.1 copy.32
  82.9 47.9 %all-to-all-done.1 = bf16[32,512,64]{1,2,0:T(8,128)(2,1)S(1)} async-done(((bf16[32,512,64]{1,2,0:T(8,128)(2,1)}), bf16[32,512,64]{1,2,0:T(8,128)(2,1)S(1)}, u32[]{:S(2)}, u32[]{:S(2)}) %all-to-all-start.1) | async-done | bytes 2097184 | tf_op jit(solution)/shard_map/all_to_all | solution.py:16
  130.9 7.4 %all-to-all-start.2 = ((bf16[128,32,64]{0,2,1:T(8,128)(2,1)}), bf16[128,32,64]{0,2,1:T(8,128)(2,1)S(1)}, u32[]{:S(2)}, u32[]{:S(2)}) async-start(bf16[128,32,64]{0,2,1:T(8,128)(2,1)} %bitcast.51), calls=%async_computation.2 | async-start | bytes 1048576 | tf_op jit(solution)/shard_map/all_to_all | solution.py:114
  138.3 2.7 fusion.18
  141.0 0.8 copy-done.6
  141.8 0.5 fusion.6
  142.3 13.3 %all-to-all-done.2 = bf16[128,32,64]{0,2,1:T(8,128)(2,1)S(1)} async-done(((bf16[128,32,64]{0,2,1:T(8,128)(2,1)}), bf16[128,32,64]{0,2,1:T(8,128)(2,1)S(1)}, u32[]{:S(2)}, u32[]{:S(2)}) %all-to-all-start.2) | async-done | bytes 524320 | tf_op jit(solution)/shard_map/all_to_all | solution.py:114
  155.6 0.8 stack.12
  156.4 4.2 all-to-all-start.3
  160.6 1.0 multiply_convert_fusion
  161.6 11.3 %all-to-all-done.3 = bf16[4,1,128,512]{3,2,1,0:T(8,128)(2,1)} async-done(((bf16[4,1,128,512]{3,2,1,0:T(8,128)(2,1)}), bf16[4,1,128,512]{3,2,1,0:T(8,128)(2,1)}, u32[]{:S(2)}, u32[]{:S(2)}) %all-to-all-start.3) | async-done | bytes 524320 | tf_op jit(solution)/shard_map/all_to_all | solution.py:42
  173.0 15.6 %all_to_all.80 = bf16[4,1,128,512]{3,2,1,0:T(8,128)(2,1)} all-to-all(bf16[4,1,128,512]{3,2,1,0:T(8,128)(2,1)S(1)} %stack.14), channel_id=1, replica_groups=mesh['rep'=2,'fs_0'=4,'fs_1'=8,'tp'=8] {'fs_0'}, dimensions={0} | all-to-all | bytes 1048576 | tf_op jit(solution)/shard_map/all_to_all | solution.py:42
  188.6 3.5 stack.13
  192.1 6.4 %all-to-all-start.4 = ((bf16[8,4,128,512]{3,2,1,0:T(8,128)(2,1)}), bf16[8,4,128,512]{3,2,1,0:T(8,128)(2,1)}, u32[]{:S(2)}, u32[]{:S(2)}) async-start(bf16[8,4,128,512]{3,2,1,0:T(8,128)(2,1)} %stack.13), calls=%async_computation.4 | async-start | bytes 8388608 | tf_op jit(solution)/shard_map/all_to_all | solution.py:42
  198.5 2.5 fusion.4
  200.9 0.9 copy.41
  201.9 0.8 fusion.3
  202.8 89.2 %all-to-all-done.4 = bf16[8,4,128,512]{3,2,1,0:T(8,128)(2,1)} async-done(((bf16[8,4,128,512]{3,2,1,0:T(8,128)(2,1)}), bf16[8,4,128,512]{3,2,1,0:T(8,128)(2,1)}, u32[]{:S(2)}, u32[]{:S(2)}) %all-to-all-start.4) | async-done | bytes 4194336 | tf_op jit(solution)/shard_map/all_to_all | solution.py:42
  292.0 3.5 stack.15
  295.5 6.2 %all-to-all-start.7 = ((bf16[8,4,128,512]{3,2,1,0:T(8,128)(2,1)}), bf16[8,4,128,512]{3,2,1,0:T(8,128)(2,1)}, u32[]{:S(2)}, u32[]{:S(2)}) async-start(bf16[8,4,128,512]{3,2,1,0:T(8,128)(2,1)} %stack.15), calls=%async_computation.7 | async-start | bytes 8388608 | tf_op jit(solution)/shard_map/all_to_all | solution.py:42
  301.7 1.0 pad_maximum_fusion
  302.9 1.0 copy.36
  303.9 93.1 %all-to-all-done.7 = bf16[8,4,128,512]{3,2,1,0:T(8,128)(2,1)} async-done(((bf16[8,4,128,512]{3,2,1,0:T(8,128)(2,1)}), bf16[8,4,128,512]{3,2,1,0:T(8,128)(2,1)}, u32[]{:S(2)}, u32[]{:S(2)}) %all-to-all-start.7) | async-done | bytes 4194336 | tf_op jit(solution)/shard_map/all_to_all | solution.py:42
  396.9 5.8 %all-to-all-start.8 = ((bf16[128,32,64]{0,2,1:T(8,128)(2,1)}), bf16[128,32,64]{0,2,1:T(8,128)(2,1)}, u32[]{:S(2)}, u32[]{:S(2)}) async-start(bf16[128,32,64]{0,2,1:T(8,128)(2,1)} %bitcast.12), calls=%async_computation.8 | async-start | bytes 1048576 | tf_op jit(solution)/shard_map/all_to_all | solution.py:113
  402.8 2.1 slice_convert_fusion
  405.0 0.3 fusion.10
  405.3 2.6 copy.34
  408.0 4.6 %copy.35 = bf16[8,4,128,512]{3,2,0,1:T(8,128)(2,1)} copy(bf16[8,4,128,512]{3,2,1,0:T(8,128)(2,1)} %all-to-all-done.7) | data formatting | bytes 8388608 | tf_op jit(solution)/shard_map/all_to_all | solution.py:42
  412.6 0.8 fusion.7
  413.4 6.5 %all-to-all-done.8 = bf16[128,32,64]{0,2,1:T(8,128)(2,1)} async-done(((bf16[128,32,64]{0,2,1:T(8,128)(2,1)}), bf16[128,32,64]{0,2,1:T(8,128)(2,1)}, u32[]{:S(2)}, u32[]{:S(2)}) %all-to-all-start.8) | async-done | bytes 524320 | tf_op jit(solution)/shard_map/all_to_all | solution.py:113
  419.9 0.7 broadcast_in_dim.10
  420.6 7.6 %all-to-all-start.5 = ((bf16[2,64,512]{2,1,0:T(8,128)(2,1)}), bf16[2,64,512]{2,1,0:T(8,128)(2,1)S(1)}, u32[]{:S(2)}, u32[]{:S(2)}) async-start(bf16[2,64,512]{2,1,0:T(8,128)(2,1)} %broadcast_in_dim.10), calls=%async_computation.5 | async-start | bytes 262144 | tf_op jit(solution)/shard_map/all_to_all | solution.py:16
  428.1 3.2 fusion.8
  431.4 5.2 %all-to-all-done.5 = bf16[2,64,512]{2,1,0:T(8,128)(2,1)S(1)} async-done(((bf16[2,64,512]{2,1,0:T(8,128)(2,1)}), bf16[2,64,512]{2,1,0:T(8,128)(2,1)S(1)}, u32[]{:S(2)}, u32[]{:S(2)}) %all-to-all-start.5) | async-done | bytes 131104 | tf_op jit(solution)/shard_map/all_to_all | solution.py:16
  436.5 0.7 broadcast_in_dim.22
  437.2 3.4 all-to-all-start.9
  440.6 1.1 fusion.13
  441.7 1.0 slice.33
  442.8 0.7 add.26
  443.4 5.5 %all-to-all-done.9 = bf16[2,512,64]{1,2,0:T(8,128)(2,1)S(1)} async-done(((bf16[2,512,64]{1,2,0:T(8,128)(2,1)}), bf16[2,512,64]{1,2,0:T(8,128)(2,1)S(1)}, u32[]{:S(2)}, u32[]{:S(2)}) %all-to-all-start.9) | async-done | bytes 131104 | tf_op jit(solution)/shard_map/all_to_all | solution.py:16
  449.0 0.7 add.27
  (33 shorter events, 0.6 us)
Async XLA Ops:
  8.2 64.3 %copy-start.11 = (bf16[512,64]{0,1:T(8,128)(2,1)S(1)}, bf16[512,64]{0,1:T(8,128)(2,1)}, u32[]{:S(2)}) copy-start(bf16[512,64]{0,1:T(8,128)(2,1)} %param.13) | copy-start | bytes 196612
  74.1 5.1 %copy-start = (bf16[128,2048]{1,0:T(8,128)(2,1)S(1)}, bf16[128,2048]{1,0:T(8,128)(2,1)}, u32[]{:S(2)}) copy-start(bf16[128,2048]{1,0:T(8,128)(2,1)} %param.9) | copy-start | bytes 1572868
  74.1 5.3 %copy-start.2 = (bf16[128,2048]{1,0:T(8,128)(2,1)S(1)}, bf16[128,2048]{1,0:T(8,128)(2,1)}, u32[]{:S(2)}) copy-start(bf16[128,2048]{1,0:T(8,128)(2,1)} %param.8) | copy-start | bytes 1572868
  74.1 5.5 %copy-start.10 = (f32[2048]{0:T(1024)S(1)}, f32[2048]{0:T(1024)}, u32[]{:S(2)}) copy-start(f32[2048]{0:T(1024)} %param.11) | copy-start | bytes 24580
  74.1 56.8 %all-to-all-start.1 = ((bf16[32,512,64]{1,2,0:T(8,128)(2,1)}), bf16[32,512,64]{1,2,0:T(8,128)(2,1)S(1)}, u32[]{:S(2)}, u32[]{:S(2)}) async-start(bf16[32,512,64]{1,2,0:T(8,128)(2,1)} %broadcast_in_dim.9), calls=%async_computation.1 | async-start | bytes 4194304 | tf_op jit(solution)/shard_map/all_to_all | solution.py:16
  130.9 24.7 %all-to-all-start.2 = ((bf16[128,32,64]{0,2,1:T(8,128)(2,1)}), bf16[128,32,64]{0,2,1:T(8,128)(2,1)S(1)}, u32[]{:S(2)}, u32[]{:S(2)}) async-start(bf16[128,32,64]{0,2,1:T(8,128)(2,1)} %bitcast.51), calls=%async_computation.2 | async-start | bytes 1048576 | tf_op jit(solution)/shard_map/all_to_all | solution.py:114
  138.3 3.5 copy-start.3
  141.0 0.8 copy-start.6
  156.4 16.5 %all-to-all-start.3 = ((bf16[4,1,128,512]{3,2,1,0:T(8,128)(2,1)}), bf16[4,1,128,512]{3,2,1,0:T(8,128)(2,1)}, u32[]{:S(2)}, u32[]{:S(2)}) async-start(bf16[4,1,128,512]{3,2,1,0:T(8,128)(2,1)} %stack.12), calls=%async_computation.3 | async-start | bytes 1048576 | tf_op jit(solution)/shard_map/all_to_all | solution.py:42
  192.1 99.9 %all-to-all-start.4 = ((bf16[8,4,128,512]{3,2,1,0:T(8,128)(2,1)}), bf16[8,4,128,512]{3,2,1,0:T(8,128)(2,1)}, u32[]{:S(2)}, u32[]{:S(2)}) async-start(bf16[8,4,128,512]{3,2,1,0:T(8,128)(2,1)} %stack.13), calls=%async_computation.4 | async-start | bytes 8388608 | tf_op jit(solution)/shard_map/all_to_all | solution.py:42
  198.5 3.4 copy-start.7
  295.5 6.2 %copy-start.5 = (bf16[16,16,8,128]{3,1,2,0:T(8,128)(2,1)S(1)}, bf16[16,16,8,128]{3,1,2,0:T(8,128)(2,1)}, u32[]{:S(2)}) copy-start(bf16[16,16,8,128]{3,1,2,0:T(8,128)(2,1)} %copy.41) | copy-start | bytes 1572868
  295.5 101.4 %all-to-all-start.7 = ((bf16[8,4,128,512]{3,2,1,0:T(8,128)(2,1)}), bf16[8,4,128,512]{3,2,1,0:T(8,128)(2,1)}, u32[]{:S(2)}, u32[]{:S(2)}) async-start(bf16[8,4,128,512]{3,2,1,0:T(8,128)(2,1)} %stack.15), calls=%async_computation.7 | async-start | bytes 8388608 | tf_op jit(solution)/shard_map/all_to_all | solution.py:42
  301.7 1.2 copy-start.4
  301.7 101.0 %all-reduce.2.cloned.1.call-start = ((), (), s32[]{:S(2)}) async-start(), calls=%async_computation.10 | async-start | bytes 2097152 | tf_op jit(solution)/shard_map/psum | solution.py:34
  396.9 22.9 %all-to-all-start.8 = ((bf16[128,32,64]{0,2,1:T(8,128)(2,1)}), bf16[128,32,64]{0,2,1:T(8,128)(2,1)}, u32[]{:S(2)}, u32[]{:S(2)}) async-start(bf16[128,32,64]{0,2,1:T(8,128)(2,1)} %bitcast.12), calls=%async_computation.8 | async-start | bytes 1048576 | tf_op jit(solution)/shard_map/all_to_all | solution.py:113
  420.6 16.0 %all-to-all-start.5 = ((bf16[2,64,512]{2,1,0:T(8,128)(2,1)}), bf16[2,64,512]{2,1,0:T(8,128)(2,1)S(1)}, u32[]{:S(2)}, u32[]{:S(2)}) async-start(bf16[2,64,512]{2,1,0:T(8,128)(2,1)} %broadcast_in_dim.10), calls=%async_computation.5 | async-start | bytes 262144 | tf_op jit(solution)/shard_map/all_to_all | solution.py:16
  431.3 10.4 %copy-start.1 = (bf16[262144]{0:T(1024)(128)(2,1)S(1)}, bf16[262144]{0:T(1024)(128)(2,1)}, u32[]{:S(2)}) copy-start(bf16[262144]{0:T(1024)(128)(2,1)} %get-tuple-element.9) | copy-start | bytes 1572868
  431.3 11.4 %copy-start.8 = (f32[64,512]{1,0:T(8,128)S(1)}, f32[64,512]{1,0:T(8,128)}, u32[]{:S(2)}) copy-start(f32[64,512]{1,0:T(8,128)} %param.14) | copy-start | bytes 393220
  437.2 11.8 %all-to-all-start.9 = ((bf16[2,512,64]{1,2,0:T(8,128)(2,1)}), bf16[2,512,64]{1,2,0:T(8,128)(2,1)S(1)}, u32[]{:S(2)}, u32[]{:S(2)}) async-start(bf16[2,512,64]{1,2,0:T(8,128)(2,1)} %broadcast_in_dim.22), calls=%async_computation.9 | async-start | bytes 262144 | tf_op jit(solution)/shard_map/all_to_all | solution.py:16
  440.6 8.4 %copy-start.9 = (f32[512,64]{0,1:T(8,128)S(1)}, f32[512,64]{0,1:T(8,128)}, u32[]{:S(2)}) copy-start(f32[512,64]{0,1:T(8,128)} %param.15) | copy-start | bytes 393220
Sparse Core Ops, SparseCore 0:
  304.9 74.4 all-reduce.1
